TPU v7x, 128 devices: a whole 4x4x4 slice. The times are simulated.
128 devices in a mesh: rep: 16 (over z, x), fs: 4 (over y), tp: 2 (over core).
Axes of the slice: x: 4, y: 4, z: 4, core: 2. Of those that a mesh axis runs over, the one named last changes fastest.
Arguments:
- tokens_in: bfloat16 [32768, 2048], P(('rep', 'fs', 'tp')), may hold values from -6 to 6
- norm_gain: float32 [2048], replicated, may hold values from 0.1 to 1.9
- gate_weight: bfloat16 [2048, 3072], P(None, ('fs', 'tp')), may hold values from -0.125 to 0.125
- up_weight: bfloat16 [2048, 3072], P(None, ('fs', 'tp')), may hold values from -0.125 to 0.125
- down_weight: bfloat16 [3072, 2048], P(('fs', 'tp')), may hold values from -0.109375 to 0.109375
- out_grad: bfloat16 [32768, 2048], P(('rep', 'fs', 'tp')), may hold values from -24 to 24
Outputs:
- grad_in: bfloat16 [32768, 2048], P(('rep', 'fs', 'tp'))
- grad_gain: float32 [2048], replicated
- grad_gate: float32 [2048, 3072], P(None, ('fs', 'tp'))
- grad_up: float32 [2048, 3072], P(None, ('fs', 'tp'))
- grad_down: float32 [3072, 2048], P(('fs', 'tp'))
All inputs are finite; a program needn't handle non-finite values.
Results may differ from a plain program's by a relative error of at most 0.014.
Values may be sent and summed in bfloat16 or wider, within the bound.
A program may use at most 192 MiB of HBM per device.

v0:
```python
import jax
import jax.numpy as jnp
from jax import lax
from jax.sharding import PartitionSpec as P

norm_eps = 1e-06


def sent_to_all(value, axis):
    length = lax.axis_size(axis)
    return lax.all_to_all(
        jnp.broadcast_to(value[None], (length, *value.shape)), axis, 0, 0, tiled=True
    )


def taken_together(value, axis):
    return sent_to_all(value, axis).sum(axis=0)


def shards(tokens_in, norm_gain, gate_weight, up_weight, down_weight, out_grad):
    row_count = tokens_in.shape[0]
    total_tokens = row_count * lax.axis_size("rep") * lax.axis_size("fs") * lax.axis_size("tp")
    factor = float(total_tokens) ** (-0.5)
    whole_in, whole_grad = (
        lax.all_gather(tokens_in, ("fs", "tp"), axis=0, tiled=True),
        lax.all_gather(out_grad, ("fs", "tp"), axis=0, tiled=True),
    )
    floats = whole_in.astype(jnp.float32)
    inverse = lax.rsqrt(jnp.mean(floats * floats, axis=-1, keepdims=True) + norm_eps)
    unit_rows = floats * inverse
    normed = (unit_rows * norm_gain).astype(jnp.bfloat16)
    gate_pre = jnp.dot(normed, gate_weight, preferred_element_type=jnp.float32)
    up_pre = jnp.dot(normed, up_weight, preferred_element_type=jnp.float32)
    sigma = jax.nn.sigmoid(gate_pre)
    active = gate_pre * sigma
    hidden = (active * up_pre).astype(jnp.bfloat16)
    grad_hidden = 0.5 * jnp.dot(whole_grad, down_weight.T, preferred_element_type=jnp.float32)
    grad_gate_pre = (grad_hidden * up_pre * sigma * (1.0 + gate_pre * (1.0 - sigma))).astype(
        jnp.bfloat16
    )
    grad_up_pre = (grad_hidden * active).astype(jnp.bfloat16)
    result = jnp.dot(grad_gate_pre, gate_weight.T, preferred_element_type=jnp.float32)
    grad_normed = lax.psum_scatter(
        (result + jnp.dot(grad_up_pre, up_weight.T, preferred_element_type=jnp.float32)).astype(
            jnp.bfloat16
        ),
        ("fs", "tp"),
        scatter_dimension=0,
        tiled=True,
    ).astype(jnp.float32)
    local_gate = jnp.dot(normed.T, grad_gate_pre, preferred_element_type=jnp.float32)
    local_up = jnp.dot(normed.T, grad_up_pre, preferred_element_type=jnp.float32)
    local_down = jnp.dot(hidden.T, whole_grad, preferred_element_type=jnp.float32)
    summed_gate = lax.psum(local_gate.astype(jnp.bfloat16), "rep").astype(jnp.float32)
    summed_up = lax.psum(local_up.astype(jnp.bfloat16), "rep").astype(jnp.float32)
    summed_down = lax.psum(local_down.astype(jnp.bfloat16), "rep").astype(jnp.float32)
    grad_gate = summed_gate * factor
    grad_up = summed_up * factor
    grad_down = summed_down * (0.5 * factor)
    position = lax.axis_index("fs") * lax.axis_size("tp") + lax.axis_index("tp")
    own_unit = lax.dynamic_slice_in_dim(unit_rows, position * row_count, row_count, 0)
    own_inverse = lax.dynamic_slice_in_dim(inverse, position * row_count, row_count, 0)
    gain_local = jnp.sum(grad_normed * own_unit, axis=0)
    gain_partial = taken_together(gain_local, ("fs", "tp"))
    grad_gain = taken_together(gain_partial, "rep")
    scaled = grad_normed * norm_gain
    grad_in = (
        out_grad.astype(jnp.float32)
        + own_inverse * scaled
        - own_unit * own_inverse * jnp.mean(scaled * own_unit, axis=-1, keepdims=True)
    )
    return (grad_in.astype(jnp.bfloat16), grad_gain, grad_gate, grad_up, grad_down)


def solution(mesh):
    in_specs = (
        P(("rep", "fs", "tp"), None),
        P(),
        P(None, ("fs", "tp")),
        P(None, ("fs", "tp")),
        P(("fs", "tp"), None),
        P(("rep", "fs", "tp"), None),
    )
    out_specs = (
        P(("rep", "fs", "tp"), None),
        P(),
        P(None, ("fs", "tp")),
        P(None, ("fs", "tp")),
        P(("fs", "tp"), None),
    )
    return jax.shard_map(shards, mesh=mesh, in_specs=in_specs, out_specs=out_specs, check_vma=False)
```

profile of v0, /device:TPU:0, one launch (start us, length us, event | category | flops | bytes accessed | tf_op | source)
XLA Modules:
  0.0 341.8 jit_solution(17009870952825740865)
XLA Ops:
  8.0 0.7 all-gather.5.cloned.1.call-update
  8.7 53.2 %all-gather.3.cloned.1.call-done = bf16[2048,2048]{1,0:T(8,128)(2,1)} async-done(((bf16[256,2048]{1,0:T(8,128)(2,1)}), bf16[2048,2048]{1,0:T(8,128)(2,1)}) %all-gather.3.cloned.1.call-update) | async-done | bytes 8388624 | tf_op jit(solution)/shard_map/all_gather | solution.py:25
  61.9 5.2 %fusion = f32[2048]{0:T(1024)S(1)} fusion(bf16[2048,2048]{1,0:T(8,128)(2,1)} %all-gather.3.cloned.1.call-done), kind=kLoop, calls=%fused_computation.2 | loop fusion | flops 12580864 | bytes 8396800 | tf_op jit(solution)/shard_map/reduce_sum | solution.py:29
  67.7 6.3 %fusion.12 = f32[2048,384]{1,0:T(8,128)} fusion(bf16[2048,384]{1,0:T(8,128)(2,1)S(1)} %copy-done.3, f32[2048]{0:T(1024)S(1)} %copy-done.9, f32[2048]{0:T(1024)S(1)} %add_rsqrt_fusion, bf16[2048,2048]{1,0:T(8,128)(2,1)S(1)} %copy-done.1), kind=kOutput, calls=%fused_computation.30 | convolution fusion | flops 3238002688 | bytes 13123584 | tf_op jit(solution)/shard_map/dot_general | solution.py:33
  74.0 6.4 %fusion.11 = f32[2048,384]{1,0:T(8,128)} fusion(bf16[2048,384]{1,0:T(8,128)(2,1)S(1)} %copy-done, f32[2048]{0:T(1024)S(1)} %copy-done.9, f32[2048]{0:T(1024)S(1)} %add_rsqrt_fusion, bf16[2048,2048]{1,0:T(8,128)(2,1)S(1)} %copy-done.1), kind=kOutput, calls=%fused_computation.29 | convolution fusion | flops 3238002688 | bytes 13123584 | tf_op jit(solution)/shard_map/dot_general | solution.py:32
  80.4 33.1 %all-gather.5.cloned.1.call-done = bf16[2048,2048]{1,0:T(8,128)(2,1)} async-done(((bf16[256,2048]{1,0:T(8,128)(2,1)}), bf16[2048,2048]{1,0:T(8,128)(2,1)}) %all-gather.5.cloned.1.call-update) | async-done | bytes 8388624 | tf_op jit(solution)/shard_map/all_gather | solution.py:26
  113.5 10.3 %convolution_convert_fusion = bf16[384,2048]{1,0:T(8,128)(2,1)} fusion(bf16[2048,2048]{1,0:T(8,128)(2,1)} %all-gather.5.cloned.1.call-done, f32[2048,384]{1,0:T(8,128)} %fusion.12, f32[2048,384]{1,0:T(8,128)} %fusion.11), kind=kOutput, calls=%fused_computation.14 | convolution fusion | flops 3226730496 | bytes 16252928 | tf_op jit(solution)/shard_map/dot_general | solution.py:53
  123.8 7.5 %multiply_convert_fusion.2 = (bf16[2048,384]{1,0:T(8,128)(2,1)S(1)}, bf16[2048,384]{1,0:T(8,128)(2,1)S(1)}) fusion(f32[2048,384]{1,0:T(8,128)} %fusion.11, f32[2048,384]{1,0:T(8,128)S(1)} %copy-done.12, bf16[2048,2048]{1,0:T(8,128)(2,1)S(1)} %copy-done.10, bf16[384,2048]{1,0:T(8,128)(2,1)S(1)} %copy-done.11), kind=kOutput, calls=%fused_computation.9 | convolution fusion | flops 3232235520 | bytes 19398656 | tf_op jit(solution)/shard_map/dot_general | solution.py:37
  131.4 6.1 %convolution_convert_fusion.1 = bf16[2048,384]{1,0:T(8,128)(2,1)} fusion(bf16[2048,384]{1,0:T(8,128)(2,1)S(1)} %get-tuple-element.10, f32[2048]{0:T(1024)S(1)} %copy-done.9, f32[2048]{0:T(1024)S(1)} %add_rsqrt_fusion, bf16[2048,2048]{1,0:T(8,128)(2,1)S(1)} %bitcast.12), kind=kOutput, calls=%fused_computation.15 | convolution fusion | flops 3238789120 | bytes 11550720 | tf_op jit(solution)/shard_map/dot_general | solution.py:52
  137.5 6.1 %convolution_convert_fusion.2 = bf16[2048,384]{1,0:T(8,128)(2,1)} fusion(bf16[2048,384]{1,0:T(8,128)(2,1)S(1)} %get-tuple-element.11, f32[2048]{0:T(1024)S(1)} %copy-done.9, f32[2048]{0:T(1024)S(1)} %add_rsqrt_fusion, bf16[2048,2048]{1,0:T(8,128)(2,1)S(1)} %bitcast.12), kind=kOutput, calls=%fused_computation.16 | convolution fusion | flops 3238789120 | bytes 11550720 | tf_op jit(solution)/shard_map/dot_general | solution.py:51
  143.8 10.1 %fusion.13 = f32[2048,2048]{1,0:T(8,128)} fusion(bf16[2048,384]{1,0:T(8,128)(2,1)} %copy-done.8, bf16[2048,384]{1,0:T(8,128)(2,1)S(1)} %copy-done), kind=kOutput, calls=%fused_computation.31 | convolution fusion | flops 3221225472 | bytes 19922944 | tf_op jit(solution)/shard_map/dot_general | solution.py:42
  153.9 10.3 %add_convert_fusion = bf16[2048,2048]{1,0:T(8,128)(2,1)} fusion(f32[2048,2048]{1,0:T(8,128)} %fusion.13, bf16[2048,384]{1,0:T(8,128)(2,1)S(1)} %copy-done.7, bf16[2048,384]{1,0:T(8,128)(2,1)S(1)} %copy-done.3), kind=kOutput, calls=%fused_computation.3 | convolution fusion | flops 3229614080 | bytes 28311552 | tf_op jit(solution)/shard_map/dot_general | solution.py:44
  164.4 10.6 %convert_multiply_fusion = f32[2048,2048]{1,0:T(8,128)} fusion(bf16[2048,2048]{1,0:T(8,128)(2,1)} %all-gather.3.cloned.1.call-done, f32[2048]{0:T(1024)S(1)} %add_rsqrt_fusion), kind=kLoop, calls=%fused_computation | loop fusion | flops 8388608 | bytes 25174016 | tf_op jit(solution)/shard_map/mul | solution.py:30
  175.0 77.3 %all-reduce.3.cloned.1.call-done = (bf16[2048,384]{1,0:T(8,128)(2,1)}, bf16[2048,384]{1,0:T(8,128)(2,1)}, bf16[384,2048]{1,0:T(8,128)(2,1)}) async-done(((bf16[2048,384]{1,0:T(8,128)(2,1)}, bf16[2048,384]{1,0:T(8,128)(2,1)}, bf16[384,2048]{1,0:T(8,128)(2,1)}), (bf16[2048,384]{1,0:T(8,128)(2,1)}, bf16[2048,384]{1,0:T(8,128)(2,1)}, bf16[384,2048]{1,0:T(8,128)(2,1)})) %all-reduce.3.cloned.1.call-update) | async-done | bytes 4718608 | tf_op jit(solution)/shard_map/psum | solution.py:54
  252.3 3.6 %convert_multiply_fusion.2 = f32[384,2048]{1,0:T(8,128)} fusion(bf16[384,2048]{1,0:T(8,128)(2,1)} %get-tuple-element.9), kind=kLoop, calls=%fused_computation.5 | loop fusion | flops 1572864 | bytes 4718592 | tf_op jit(solution)/shard_map/mul | solution.py:59
  255.9 3.3 convert_multiply_fusion.3
  259.2 47.5 %reduce-scatter.2.cloned.1.call-done = bf16[256,2048]{1,0:T(8,128)(2,1)} async-done(((bf16[2048,2048]{1,0:T(8,128)(2,1)}), bf16[256,2048]{1,0:T(8,128)(2,1)}) %reduce-scatter.2.cloned.1.call-update) | async-done | bytes 1048592 | tf_op jit(solution)/shard_map/reduce_scatter | solution.py:43
  306.7 2.6 fusion.8
  309.9 3.4 all-to-all-start
  313.3 5.5 %all-to-all-done = f32[8,1,2048]{2,1,0:T(1,128)S(1)} async-done(((f32[8,1,2048]{2,1,0:T(1,128)}), f32[8,1,2048]{2,1,0:T(1,128)S(1)}, u32[]{:S(2)}, u32[]{:S(2)}) %all-to-all-start) | async-done | bytes 65568 | tf_op jit(solution)/shard_map/all_to_all | solution.py:11
  318.9 0.7 broadcast_in_dim.5
  319.6 6.9 %all-to-all-start.1 = ((f32[16,1,2048]{2,1,0:T(1,128)}), f32[16,1,2048]{2,1,0:T(1,128)S(1)}, u32[]{:S(2)}, u32[]{:S(2)}) async-start(f32[16,1,2048]{2,1,0:T(1,128)} %broadcast_in_dim.5), calls=%async_computation.2 | async-start | bytes 262144 | tf_op jit(solution)/shard_map/all_to_all | solution.py:11
  326.6 3.6 %fusion.6 = bf16[256,2048]{1,0:T(8,128)(2,1)} fusion(bf16[256,2048]{1,0:T(8,128)(2,1)} %reduce-scatter.2.cloned.1.call-done, bf16[256,2048]{1,0:T(8,128)(2,1)S(1)} %copy-done.2, f32[2048,2048]{1,0:T(8,128)} %convert_multiply_fusion, s32[]{:T(128)S(6)} %select_n.4, f32[256]{0:T(256)S(1)} %broadcast_multiply_fusion, f32[2048]{0:T(1024)S(1)} %copy-done.9, ...), kind=kLoop, calls=%fused_computation.23 | loop fusion | flops 4718592 | bytes 5253124 | tf_op jit(solution)/shard_map/convert_element_type | solution.py:72
  330.1 4.4 %all-to-all-done.1 = f32[16,1,2048]{2,1,0:T(1,128)S(1)} async-done(((f32[16,1,2048]{2,1,0:T(1,128)}), f32[16,1,2048]{2,1,0:T(1,128)S(1)}, u32[]{:S(2)}, u32[]{:S(2)}) %all-to-all-start.1) | async-done | bytes 131104 | tf_op jit(solution)/shard_map/all_to_all | solution.py:11
  (44 shorter events, 3.1 us)
Async XLA Ops:
  7.2 66.8 %copy-start = (bf16[2048,384]{1,0:T(8,128)(2,1)S(1)}, bf16[2048,384]{1,0:T(8,128)(2,1)}, u32[]{:S(2)}) copy-start(bf16[2048,384]{1,0:T(8,128)(2,1)} %param.8) | copy-start | bytes 4718596
  7.2 54.7 %all-gather.3.cloned.1.call-start = ((), (), s32[]{:S(2)}) async-start(), calls=%async_computation.3 | async-start | bytes 9437184 | tf_op jit(solution)/shard_map/all_gather | solution.py:25
  7.2 59.9 %copy-start.3 = (bf16[2048,384]{1,0:T(8,128)(2,1)S(1)}, bf16[2048,384]{1,0:T(8,128)(2,1)}, u32[]{:S(2)}) copy-start(bf16[2048,384]{1,0:T(8,128)(2,1)} %param.9) | copy-start | bytes 4718596
  7.9 105.6 %all-gather.5.cloned.1.call-start = ((), (), s32[]{:S(2)}) async-start(), calls=%async_computation.4 | async-start | bytes 9437184 | tf_op jit(solution)/shard_map/all_gather | solution.py:26
  8.7 58.5 %copy-start.9 = (f32[2048]{0:T(1024)S(1)}, f32[2048]{0:T(1024)}, u32[]{:S(2)}) copy-start(f32[2048]{0:T(1024)} %param.7) | copy-start | bytes 24580
  8.7 243.6 %all-reduce.3.cloned.1.call-start = ((), (), s32[]{:S(2)}) async-start(), calls=%async_computation.6 | async-start | bytes 9437184 | tf_op jit(solution)/shard_map/psum | solution.py:54
  61.9 5.8 %copy-start.1 = (bf16[2048,2048]{1,0:T(8,128)(2,1)S(1)}, bf16[2048,2048]{1,0:T(8,128)(2,1)}, u32[]{:S(2)}) copy-start(bf16[2048,2048]{1,0:T(8,128)(2,1)} %all-gather.3.cloned.1.call-done) | copy-start | bytes 25165828
  113.5 10.4 %copy-start.10 = (bf16[2048,2048]{1,0:T(8,128)(2,1)S(1)}, bf16[2048,2048]{1,0:T(8,128)(2,1)}, u32[]{:S(2)}) copy-start(bf16[2048,2048]{1,0:T(8,128)(2,1)} %all-gather.5.cloned.1.call-done) | copy-start | bytes 25165828
  113.5 10.4 %copy-start.11 = (bf16[384,2048]{1,0:T(8,128)(2,1)S(1)}, bf16[384,2048]{1,0:T(8,128)(2,1)}, u32[]{:S(2)}) copy-start(bf16[384,2048]{1,0:T(8,128)(2,1)} %param.10) | copy-start | bytes 4718596
  113.5 10.4 %copy-start.12 = (f32[2048,384]{1,0:T(8,128)S(1)}, f32[2048,384]{1,0:T(8,128)}, u32[]{:S(2)}) copy-start(f32[2048,384]{1,0:T(8,128)} %fusion.12) | copy-start | bytes 9437188
  113.5 17.9 %slice-start = ((s8[8388608]{0:T(1024)(128)(4,1)}), s8[4194304]{0:T(1024)(128)(4,1)S(1)}, s32[]{:S(2)}) async-start(s8[8388608]{0:T(1024)(128)(4,1)} %bitcast.11), calls=%async_computation.7 | async-start | bytes 8388608
  123.8 7.5 %slice-start.1 = ((s8[8388608]{0:T(1024)(128)(4,1)}), s8[4194304]{0:T(1024)(128)(4,1)S(1)}, s32[]{:S(2)}) async-start(s8[8388608]{0:T(1024)(128)(4,1)} %bitcast.11), calls=%async_computation.8 | async-start | bytes 8388608
  131.3 6.1 %copy-start.6 = (bf16[2048,384]{1,0:T(8,128)(2,1)}, bf16[2048,384]{1,0:T(8,128)(2,1)S(1)}, u32[]{:S(2)}) copy-start(bf16[2048,384]{1,0:T(8,128)(2,1)S(1)} %get-tuple-element.10) | copy-start | bytes 4718596
  131.3 6.1 %copy-start.8 = (bf16[2048,384]{1,0:T(8,128)(2,1)}, bf16[2048,384]{1,0:T(8,128)(2,1)S(1)}, u32[]{:S(2)}) copy-start(bf16[2048,384]{1,0:T(8,128)(2,1)S(1)} %get-tuple-element.11) | copy-start | bytes 4718596
  143.6 163.1 %reduce-scatter.2.cloned.1.call-start = ((), (), s32[]{:S(2)}) async-start(), calls=%async_computation.5 | async-start | bytes 9437184 | tf_op jit(solution)/shard_map/reduce_scatter | solution.py:43
  143.8 10.1 %copy-start.7 = (bf16[2048,384]{1,0:T(8,128)(2,1)S(1)}, bf16[2048,384]{1,0:T(8,128)(2,1)}, u32[]{:S(2)}) copy-start(bf16[2048,384]{1,0:T(8,128)(2,1)} %copy-done.6) | copy-start | bytes 4718596
  252.3 3.6 %copy-start.4 = (bf16[2048,384]{1,0:T(8,128)(2,1)S(1)}, bf16[2048,384]{1,0:T(8,128)(2,1)}, u32[]{:S(2)}) copy-start(bf16[2048,384]{1,0:T(8,128)(2,1)} %get-tuple-element.7) | copy-start | bytes 4718596
  252.3 3.6 %copy-start.5 = (bf16[2048,384]{1,0:T(8,128)(2,1)S(1)}, bf16[2048,384]{1,0:T(8,128)(2,1)}, u32[]{:S(2)}) copy-start(bf16[2048,384]{1,0:T(8,128)(2,1)} %get-tuple-element.8) | copy-start | bytes 4718596
  259.1 67.4 %copy-start.2 = (bf16[256,2048]{1,0:T(8,128)(2,1)S(1)}, bf16[256,2048]{1,0:T(8,128)(2,1)}, u32[]{:S(2)}) copy-start(bf16[256,2048]{1,0:T(8,128)(2,1)} %param.11) | copy-start | bytes 3145732
  309.9 8.9 %all-to-all-start = ((f32[8,1,2048]{2,1,0:T(1,128)}), f32[8,1,2048]{2,1,0:T(1,128)S(1)}, u32[]{:S(2)}, u32[]{:S(2)}) async-start(f32[8,1,2048]{2,1,0:T(1,128)} %broadcast_in_dim.4), calls=%async_computation.1 | async-start | bytes 131072 | tf_op jit(solution)/shard_map/all_to_all | solution.py:11
  319.6 14.9 %all-to-all-start.1 = ((f32[16,1,2048]{2,1,0:T(1,128)}), f32[16,1,2048]{2,1,0:T(1,128)S(1)}, u32[]{:S(2)}, u32[]{:S(2)}) async-start(f32[16,1,2048]{2,1,0:T(1,128)} %broadcast_in_dim.5), calls=%async_computation.2 | async-start | bytes 262144 | tf_op jit(solution)/shard_map/all_to_all | solution.py:11
Sparse Core Ops, SparseCore 0:
  9.7 52.1 all-gather.2
  63.6 49.8 all-gather.4
  143.7 108.5 all-reduce.2
  254.5 52.1 reduce-scatter.1
where the time goes:
time: 342 us
  waiting for transfers between devices  222 us (65%)
  matrix products  63.1 us (18%)
  other arithmetic  29.6 us (9%)
  between operations  13.9 us (4%)
  starting transfers between devices  10.7 us (3%)
    psum x1, waiting for transfers between devices, shards(): lax.psum(local_gate.astype(jnp.bfloat16), 'rep').astype(jnp.float32)  77.3 us
    all_gather x1, waiting for transfers between devices, shards(): lax.all_gather(tokens_in, ('fs', 'tp'), axis=0, tiled=True)  53.2 us
    reduce_scatter x1, waiting for transfers between devices, shards(): lax.psum_scatter((result + jnp.dot(grad_up_pre, up_weight.T, preferred_el...  47.5 us
    all_gather x1, waiting for transfers between devices, shards(): lax.all_gather(out_grad, ('fs', 'tp'), axis=0, tiled=True)  33.1 us
    mul x1, other arithmetic, shards(): unit_rows = floats * inverse  10.6 us
    dot_general x1, matrix products, shards(): jnp.dot(hidden.T, whole_grad, preferred_element_type=jnp.float32)  10.3 us
    dot_general x1, matrix products, shards(): jnp.dot(grad_up_pre, up_weight.T, preferred_element_type=jnp.float32)  10.3 us
    all_to_all x2, starting transfers between devices, sent_to_all(): lax.all_to_all(jnp.broadcast_to(value[None], (length, *value.shape)), axi...  10.3 us
  transfers between devices with their start and end apart: 6, of which 6 were waited for; matrix products, arithmetic and copies ran while one was open for 17% of the time, Pallas kernels for 0%

commit v1 on v0

--- a/solution.py
+++ b/solution.py
@@ -51,7 +51,9 @@
     local_gate = jnp.dot(normed.T, grad_gate_pre, preferred_element_type=jnp.float32)
     local_up = jnp.dot(normed.T, grad_up_pre, preferred_element_type=jnp.float32)
     local_down = jnp.dot(hidden.T, whole_grad, preferred_element_type=jnp.float32)
-    summed_gate = lax.psum(local_gate.astype(jnp.bfloat16), "rep").astype(jnp.float32)
+    summed_gate = jnp.sum(lax.all_gather(local_gate.astype(jnp.bfloat16), "rep"), axis=0).astype(
+        jnp.float32
+    )
     summed_up = lax.psum(local_up.astype(jnp.bfloat16), "rep").astype(jnp.float32)
     summed_down = lax.psum(local_down.astype(jnp.bfloat16), "rep").astype(jnp.float32)
     grad_gate = summed_gate * factor

time: 342 us -> 470 us (1.37)
  waiting for transfers between devices: 222 us -> 330 us
  other arithmetic: 29.6 us -> 43 us
    all_gather x0 -> x1, waiting for transfers between devices: none -> 128 us  [shards(): lax.all_gather(local_gate.astype(jnp.bfloat16), 'rep')]
    psum x1, waiting for transfers between devices: 77.3 us -> 54.5 us  [shards(): lax.psum(local_up.astype(jnp.bfloat16), 'rep').astype(jnp.float32)]
    reduce_sum x0 -> x1, other arithmetic: none -> 13.2 us  [shards(): jnp.sum(lax.all_gather(local_gate.astype(jnp.bfloat16), 'rep'), axis=0)]
  transfers between devices with their start and end apart: 6 -> 7, of which waited for: 6 -> 7; matrix products, arithmetic and copies ran while one was open for 17% -> 15% of each run, Pallas kernels for 0% -> 0%
where the time goes in v1:
time: 470 us; the launch traced here: 469 us
  waiting for transfers between devices  330 us (70%)
  matrix products  67.3 us (14%)
  other arithmetic  43 us (9%)
  between operations  13.9 us (3%)
  starting transfers between devices  10.7 us (2%)
    all_gather x1, waiting for transfers between devices, shards(): lax.all_gather(local_gate.astype(jnp.bfloat16), 'rep')  128 us
    psum x1, waiting for transfers between devices, shards(): lax.psum(local_up.astype(jnp.bfloat16), 'rep').astype(jnp.float32)  54.5 us
    all_gather x1, waiting for transfers between devices, shards(): lax.all_gather(tokens_in, ('fs', 'tp'), axis=0, tiled=True)  53.2 us
    reduce_scatter x1, waiting for transfers between devices, shards(): lax.psum_scatter((result + jnp.dot(grad_up_pre, up_weight.T, preferred_el...  48.1 us
    all_gather x1, waiting for transfers between devices, shards(): lax.all_gather(out_grad, ('fs', 'tp'), axis=0, tiled=True)  33.1 us
    reduce_sum x1, other arithmetic, shards(): jnp.sum(lax.all_gather(local_gate.astype(jnp.bfloat16), 'rep'), axis=0)  13.2 us
    all_to_all x2, waiting for transfers between devices, sent_to_all(): lax.all_to_all(jnp.broadcast_to(value[None], (length, *value.shape)), axi...  11.9 us
    mul x1, other arithmetic, shards(): unit_rows = floats * inverse  10.4 us
  transfers between devices with their start and end apart: 7, of which 7 were waited for; matrix products, arithmetic and copies ran while one was open for 15% of the time, Pallas kernels for 0%

profile of v1, /device:TPU:0, one launch (start us, length us, event | category | flops | bytes accessed | tf_op | source)
XLA Modules:
  0.0 468.9 jit_solution(5163309298973068380)
XLA Ops:
  8.7 53.2 %all-gather.5.cloned.1.call-done = bf16[2048,2048]{1,0:T(8,128)(2,1)} async-done(((bf16[256,2048]{1,0:T(8,128)(2,1)}), bf16[2048,2048]{1,0:T(8,128)(2,1)}) %all-gather.5.cloned.1.call-update) | async-done | bytes 8388624 | tf_op jit(solution)/shard_map/all_gather | solution.py:25
  61.9 5.2 %fusion = f32[2048]{0:T(1024)S(1)} fusion(bf16[2048,2048]{1,0:T(8,128)(2,1)} %all-gather.5.cloned.1.call-done), kind=kLoop, calls=%fused_computation.2 | loop fusion | flops 12580864 | bytes 8396800 | tf_op jit(solution)/shard_map/reduce_sum | solution.py:29
  67.7 6.4 %fusion.12 = f32[2048,384]{1,0:T(8,128)} fusion(bf16[2048,384]{1,0:T(8,128)(2,1)S(1)} %copy-done.5, f32[2048]{0:T(1024)S(1)} %copy-done.10, f32[2048]{0:T(1024)S(1)} %add_rsqrt_fusion, bf16[2048,2048]{1,0:T(8,128)(2,1)S(1)} %copy-done.2), kind=kOutput, calls=%fused_computation.30 | convolution fusion | flops 3238002688 | bytes 13123584 | tf_op jit(solution)/shard_map/dot_general | solution.py:33
  74.0 6.3 %fusion.11 = f32[2048,384]{1,0:T(8,128)} fusion(bf16[2048,384]{1,0:T(8,128)(2,1)S(1)} %copy-done, f32[2048]{0:T(1024)S(1)} %copy-done.10, f32[2048]{0:T(1024)S(1)} %add_rsqrt_fusion, bf16[2048,2048]{1,0:T(8,128)(2,1)S(1)} %copy-done.2), kind=kOutput, calls=%fused_computation.29 | convolution fusion | flops 3238002688 | bytes 13123584 | tf_op jit(solution)/shard_map/dot_general | solution.py:32
  80.4 33.1 %all-gather.7.cloned.1.call-done = bf16[2048,2048]{1,0:T(8,128)(2,1)} async-done(((bf16[256,2048]{1,0:T(8,128)(2,1)}), bf16[2048,2048]{1,0:T(8,128)(2,1)}) %all-gather.7.cloned.1.call-update) | async-done | bytes 8388624 | tf_op jit(solution)/shard_map/all_gather | solution.py:26
  113.5 10.4 %convolution_convert_fusion = bf16[384,2048]{1,0:T(8,128)(2,1)} fusion(bf16[2048,2048]{1,0:T(8,128)(2,1)} %all-gather.7.cloned.1.call-done, f32[2048,384]{1,0:T(8,128)} %fusion.12, f32[2048,384]{1,0:T(8,128)} %fusion.11), kind=kOutput, calls=%fused_computation.14 | convolution fusion | flops 3226730496 | bytes 16252928 | tf_op jit(solution)/shard_map/dot_general | solution.py:53
  123.9 8.3 %multiply_convert_fusion.2 = (bf16[2048,384]{1,0:T(8,128)(2,1)S(1)}, bf16[2048,384]{1,0:T(8,128)(2,1)}) fusion(f32[2048,384]{1,0:T(8,128)} %fusion.11, f32[2048,384]{1,0:T(8,128)S(1)} %copy-done.13, bf16[2048,2048]{1,0:T(8,128)(2,1)S(1)} %copy-done.11, bf16[384,2048]{1,0:T(8,128)(2,1)S(1)} %copy-done.12), kind=kOutput, calls=%fused_computation.9 | convolution fusion | flops 3232235520 | bytes 19398656 | tf_op jit(solution)/shard_map/dot_general | solution.py:37
  133.3 6.1 %convolution_convert_fusion.1 = bf16[2048,384]{1,0:T(8,128)(2,1)} fusion(bf16[2048,384]{1,0:T(8,128)(2,1)S(1)} %get-tuple-element.9, f32[2048]{0:T(1024)S(1)} %copy-done.10, f32[2048]{0:T(1024)S(1)} %add_rsqrt_fusion, bf16[2048,2048]{1,0:T(8,128)(2,1)S(1)} %bitcast.13), kind=kOutput, calls=%fused_computation.15 | convolution fusion | flops 3238789120 | bytes 11550720 | tf_op jit(solution)/shard_map/dot_general | solution.py:52
  139.5 9.9 %fusion.13 = f32[2048,2048]{1,0:T(8,128)} fusion(bf16[2048,384]{1,0:T(8,128)(2,1)} %get-tuple-element.10, bf16[2048,384]{1,0:T(8,128)(2,1)S(1)} %copy-done), kind=kOutput, calls=%fused_computation.31 | convolution fusion | flops 3221225472 | bytes 19922944 | tf_op jit(solution)/shard_map/dot_general | solution.py:42
  149.4 10.3 %add_convert_fusion = bf16[2048,2048]{1,0:T(8,128)(2,1)} fusion(f32[2048,2048]{1,0:T(8,128)} %fusion.13, bf16[2048,384]{1,0:T(8,128)(2,1)S(1)} %copy-done.8, bf16[2048,384]{1,0:T(8,128)(2,1)S(1)} %copy-done.5), kind=kOutput, calls=%fused_computation.3 | convolution fusion | flops 3229614080 | bytes 28311552 | tf_op jit(solution)/shard_map/dot_general | solution.py:44
  161.1 9.6 %convolution_convert_fusion.2 = bf16[2048,384]{1,0:T(8,128)(2,1)} fusion(bf16[2048,384]{1,0:T(8,128)(2,1)S(1)} %copy-done.6, f32[2048]{0:T(1024)S(1)} %copy-done.10, f32[2048]{0:T(1024)S(1)} %add_rsqrt_fusion, bf16[2048,2048]{1,0:T(8,128)(2,1)} %all-gather.5.cloned.1.call-done), kind=kOutput, calls=%fused_computation.16 | convolution fusion | flops 3238789120 | bytes 11550720 | tf_op jit(solution)/shard_map/dot_general | solution.py:51
  170.9 10.4 %convert_multiply_fusion = f32[2048,2048]{1,0:T(8,128)} fusion(bf16[2048,2048]{1,0:T(8,128)(2,1)} %all-gather.5.cloned.1.call-done, f32[2048]{0:T(1024)S(1)} %add_rsqrt_fusion), kind=kLoop, calls=%fused_computation | loop fusion | flops 8388608 | bytes 25174016 | tf_op jit(solution)/shard_map/mul | solution.py:30
  181.3 54.5 %all-reduce.3.cloned.1.call-done = (bf16[2048,384]{1,0:T(8,128)(2,1)}, bf16[384,2048]{1,0:T(8,128)(2,1)}) async-done(((bf16[2048,384]{1,0:T(8,128)(2,1)}, bf16[384,2048]{1,0:T(8,128)(2,1)}), (bf16[2048,384]{1,0:T(8,128)(2,1)}, bf16[384,2048]{1,0:T(8,128)(2,1)})) %all-reduce.3.cloned.1.call-update) | async-done | bytes 3145744 | tf_op jit(solution)/shard_map/psum | solution.py:57
  235.8 3.6 convert_multiply_fusion.2
  241.3 48.1 %reduce-scatter.2.cloned.1.call-done = bf16[256,2048]{1,0:T(8,128)(2,1)} async-done(((bf16[2048,2048]{1,0:T(8,128)(2,1)}), bf16[256,2048]{1,0:T(8,128)(2,1)}) %reduce-scatter.2.cloned.1.call-update) | async-done | bytes 1048592 | tf_op jit(solution)/shard_map/reduce_scatter | solution.py:43
  289.4 2.6 fusion.8
  292.7 3.4 all-to-all-start
  296.0 5.5 %all-to-all-done = f32[8,1,2048]{2,1,0:T(1,128)S(1)} async-done(((f32[8,1,2048]{2,1,0:T(1,128)}), f32[8,1,2048]{2,1,0:T(1,128)S(1)}, u32[]{:S(2)}, u32[]{:S(2)}) %all-to-all-start) | async-done | bytes 65568 | tf_op jit(solution)/shard_map/all_to_all | solution.py:11
  302.3 6.9 %all-to-all-start.1 = ((f32[16,1,2048]{2,1,0:T(1,128)}), f32[16,1,2048]{2,1,0:T(1,128)S(1)}, u32[]{:S(2)}, u32[]{:S(2)}) async-start(f32[16,1,2048]{2,1,0:T(1,128)} %broadcast_in_dim.5), calls=%async_computation.2 | async-start | bytes 262144 | tf_op jit(solution)/shard_map/all_to_all | solution.py:11
  309.3 3.3 fusion.6
  312.6 6.3 %all-to-all-done.1 = f32[16,1,2048]{2,1,0:T(1,128)S(1)} async-done(((f32[16,1,2048]{2,1,0:T(1,128)}), f32[16,1,2048]{2,1,0:T(1,128)S(1)}, u32[]{:S(2)}, u32[]{:S(2)}) %all-to-all-start.1) | async-done | bytes 131104 | tf_op jit(solution)/shard_map/all_to_all | solution.py:11
  319.6 127.6 %all-gather.9.cloned.1.call-done = bf16[32768,384]{1,0:T(8,128)(2,1)} async-done(((bf16[2048,384]{1,0:T(8,128)(2,1)}), bf16[32768,384]{1,0:T(8,128)(2,1)}) %all-gather.9.cloned.1.call-update) | async-done | bytes 25165840 | tf_op jit(solution)/shard_map/all_gather | solution.py:54
  447.2 13.2 %reduce_sum.62 = bf16[2048,384]{1,0:T(8,128)(2,1)S(1)} reduce(bf16[16,2048,384]{2,1,0:T(8,128)(2,1)} %bitcast.14, bf16[]{:T(256)} %constant.32.clone.1), dimensions={0}, to_apply=%region_6.0 | reduce | flops 11796480 | bytes 26738690 | tf_op jit(solution)/shard_map/reduce_sum | solution.py:54
  460.4 1.9 convert_multiply_fusion.4
  (51 shorter events, 8.9 us)
Async XLA Ops:
  7.2 66.9 %copy-start = (bf16[2048,384]{1,0:T(8,128)(2,1)S(1)}, bf16[2048,384]{1,0:T(8,128)(2,1)}, u32[]{:S(2)}) copy-start(bf16[2048,384]{1,0:T(8,128)(2,1)} %param.8) | copy-start | bytes 4718596
  7.2 54.7 %all-gather.5.cloned.1.call-start = ((), (), s32[]{:S(2)}) async-start(), calls=%async_computation.3 | async-start | bytes 9437184 | tf_op jit(solution)/shard_map/all_gather | solution.py:25
  7.2 59.9 %copy-start.5 = (bf16[2048,384]{1,0:T(8,128)(2,1)S(1)}, bf16[2048,384]{1,0:T(8,128)(2,1)}, u32[]{:S(2)}) copy-start(bf16[2048,384]{1,0:T(8,128)(2,1)} %param.9) | copy-start | bytes 4718596
  7.9 105.6 %all-gather.7.cloned.1.call-start = ((), (), s32[]{:S(2)}) async-start(), calls=%async_computation.4 | async-start | bytes 9437184 | tf_op jit(solution)/shard_map/all_gather | solution.py:26
  8.7 58.5 %copy-start.10 = (f32[2048]{0:T(1024)S(1)}, f32[2048]{0:T(1024)}, u32[]{:S(2)}) copy-start(f32[2048]{0:T(1024)} %param.7) | copy-start | bytes 24580
  8.7 227.1 %all-reduce.3.cloned.1.call-start = ((), (), s32[]{:S(2)}) async-start(), calls=%async_computation.7 | async-start | bytes 6291456 | tf_op jit(solution)/shard_map/psum | solution.py:57
  61.9 5.8 %copy-start.2 = (bf16[2048,2048]{1,0:T(8,128)(2,1)S(1)}, bf16[2048,2048]{1,0:T(8,128)(2,1)}, u32[]{:S(2)}) copy-start(bf16[2048,2048]{1,0:T(8,128)(2,1)} %all-gather.5.cloned.1.call-done) | copy-start | bytes 25165828
  113.5 10.4 %copy-start.11 = (bf16[2048,2048]{1,0:T(8,128)(2,1)S(1)}, bf16[2048,2048]{1,0:T(8,128)(2,1)}, u32[]{:S(2)}) copy-start(bf16[2048,2048]{1,0:T(8,128)(2,1)} %all-gather.7.cloned.1.call-done) | copy-start | bytes 25165828
  113.5 10.4 %copy-start.12 = (bf16[384,2048]{1,0:T(8,128)(2,1)S(1)}, bf16[384,2048]{1,0:T(8,128)(2,1)}, u32[]{:S(2)}) copy-start(bf16[384,2048]{1,0:T(8,128)(2,1)} %param.10) | copy-start | bytes 4718596
  113.5 10.4 %copy-start.13 = (f32[2048,384]{1,0:T(8,128)S(1)}, f32[2048,384]{1,0:T(8,128)}, u32[]{:S(2)}) copy-start(f32[2048,384]{1,0:T(8,128)} %fusion.12) | copy-start | bytes 9437188
  113.5 19.9 %slice-start = ((s8[8388608]{0:T(1024)(128)(4,1)}), s8[4194304]{0:T(1024)(128)(4,1)S(1)}, s32[]{:S(2)}) async-start(s8[8388608]{0:T(1024)(128)(4,1)} %bitcast.12), calls=%async_computation.8 | async-start | bytes 8388608
  123.9 9.5 %slice-start.1 = ((s8[8388608]{0:T(1024)(128)(4,1)}), s8[4194304]{0:T(1024)(128)(4,1)S(1)}, s32[]{:S(2)}) async-start(s8[8388608]{0:T(1024)(128)(4,1)} %bitcast.12), calls=%async_computation.9 | async-start | bytes 8388608
  132.2 1.1 copy-start.7
  139.4 149.9 %reduce-scatter.2.cloned.1.call-start = ((), (), s32[]{:S(2)}) async-start(), calls=%async_computation.5 | async-start | bytes 9437184 | tf_op jit(solution)/shard_map/reduce_scatter | solution.py:43
  139.5 9.9 %copy-start.8 = (bf16[2048,384]{1,0:T(8,128)(2,1)S(1)}, bf16[2048,384]{1,0:T(8,128)(2,1)}, u32[]{:S(2)}) copy-start(bf16[2048,384]{1,0:T(8,128)(2,1)} %copy-done.7) | copy-start | bytes 4718596
  159.7 1.4 copy-start.6
  159.7 287.5 %all-gather.9.cloned.1.call-start = ((), (), s32[]{:S(2)}) async-start(), calls=%async_computation.6 | async-start | bytes 26738688 | tf_op jit(solution)/shard_map/all_gather | solution.py:54
  235.8 3.6 copy-start.9
  239.3 70.0 %copy-start.3 = (bf16[256,2048]{1,0:T(8,128)(2,1)S(1)}, bf16[256,2048]{1,0:T(8,128)(2,1)}, u32[]{:S(2)}) copy-start(bf16[256,2048]{1,0:T(8,128)(2,1)} %param.11) | copy-start | bytes 3145732
  289.3 20.0 %copy-start.4 = (bf16[256,2048]{1,0:T(8,128)(2,1)S(1)}, bf16[256,2048]{1,0:T(8,128)(2,1)}, u32[]{:S(2)}) copy-start(bf16[256,2048]{1,0:T(8,128)(2,1)} %reduce-scatter.2.cloned.1.call-done) | copy-start | bytes 3145732
  292.7 8.9 %all-to-all-start = ((f32[8,1,2048]{2,1,0:T(1,128)}), f32[8,1,2048]{2,1,0:T(1,128)S(1)}, u32[]{:S(2)}, u32[]{:S(2)}) async-start(f32[8,1,2048]{2,1,0:T(1,128)} %broadcast_in_dim.4), calls=%async_computation.1 | async-start | bytes 131072 | tf_op jit(solution)/shard_map/all_to_all | solution.py:11
  302.3 16.6 %all-to-all-start.1 = ((f32[16,1,2048]{2,1,0:T(1,128)}), f32[16,1,2048]{2,1,0:T(1,128)S(1)}, u32[]{:S(2)}, u32[]{:S(2)}) async-start(f32[16,1,2048]{2,1,0:T(1,128)} %broadcast_in_dim.5), calls=%async_computation.2 | async-start | bytes 262144 | tf_op jit(solution)/shard_map/all_to_all | solution.py:11
  447.2 15.2 %copy-start.1 = (bf16[2048,384]{1,0:T(8,128)(2,1)S(1)}, bf16[2048,384]{1,0:T(8,128)(2,1)}, u32[]{:S(2)}) copy-start(bf16[2048,384]{1,0:T(8,128)(2,1)} %param.8) | copy-start | bytes 4718596
Sparse Core Ops, SparseCore 0:
  9.7 52.1 all-gather.4
  63.6 49.8 all-gather.6
  139.6 96.1 all-reduce.2
  238.0 51.2 reduce-scatter.1
  291.9 155.2 all-gather.8
